TPU v7x, 32 devices: a whole 2x2x4 slice. The times are simulated.
32 devices in a mesh: grp: 2 (over y), ep: 8 (over z, x), tp: 2 (over core).
Axes of the slice: x: 2, y: 2, z: 4, core: 2. Of those that a mesh axis runs over, the one named last changes fastest.
Arguments:
- fresh_inputs: bfloat16 [256, 2048], P(('grp', 'ep')), parts along dimension 0, may hold values from -6 to 6
- memory_arrays: float32 [256, 32, 64, 64], P(('grp', 'ep'), 'tp'), parts along dimension 0, may hold values from -4 to 4
- chosen_specialist: int32 [256, 2], P(('grp', 'ep')), parts along dimension 0, may hold values from 0 to 3, all different within a row; in each aligned block of 128 rows (0 to 127, 128 to 255, ...) at most 96 rows name the same one
- chosen_coefficient: bfloat16 [256, 2], P(('grp', 'ep')), parts along dimension 0, may hold values from 0.25 to 1
- first_rescale: float32 [2048], replicated, may hold values from 0.1 to 1.9
- second_rescale: float32 [2048], replicated, may hold values from 0.1 to 1.9
- receiver_projector: bfloat16 [2048, 2048], P('tp', 'ep'), may hold values from -0.125 to 0.125
- address_projector: bfloat16 [2048, 2048], P('tp', 'ep'), may hold values from -0.125 to 0.125
- content_projector: bfloat16 [2048, 2048], P('tp', 'ep'), may hold values from -0.125 to 0.125
- final_projector: bfloat16 [2048, 2048], P('tp', 'ep'), may hold values from -0.125 to 0.125
- forget_narrowing: bfloat16 [2048, 64], replicated, may hold values from -0.125 to 0.125
- forget_widening: bfloat16 [64, 2048], P(None, 'tp'), may hold values from -0.75 to 0.75
- forget_bias: float32 [2048], P('tp'), may hold values from -3 to 1
- learning_narrowing: bfloat16 [2048, 64], replicated, may hold values from -0.125 to 0.125
- learning_widening: bfloat16 [64, 2048], P(None, 'tp'), may hold values from -0.75 to 0.75
- learning_bias: float32 [2048], P('tp'), may hold values from -1.5 to 1.5
- lane_scaling: float32 [2048], P('tp'), may hold values from 0.1 to 1.9
- instant_reward: float32 [32, 64], P('tp'), may hold values from -0.5 to 0.5
- specialist_switch: bfloat16 [2048, 28672], P(None, ('ep', 'tp')), may hold values from -0.125 to 0.125
- specialist_expand: bfloat16 [2048, 28672], P(None, ('ep', 'tp')), may hold values from -0.125 to 0.125
- specialist_contract: bfloat16 [28672, 2048], P(('ep', 'tp')), may hold values from -0.0625 to 0.0625
- common_activator: bfloat16 [2048, 5632], P(None, ('ep', 'tp')), may hold values from -0.125 to 0.125
- common_expand: bfloat16 [2048, 5632], P(None, ('ep', 'tp')), may hold values from -0.125 to 0.125
- common_contract: bfloat16 [5632, 2048], P(('ep', 'tp')), may hold values from -0.078125 to 0.078125
- common_switch: bfloat16 [2048], replicated, may hold values from -0.125 to 0.125
Outputs:
- new_tokens: bfloat16 [256, 2048], P(('grp', 'ep', 'tp')), parts along dimension 0
- memory_after: float32 [256, 32, 64, 64], P(('grp', 'ep'), 'tp'), parts along dimension 0
There are 2 independent parts, one for each index of `grp`. A program takes and returns all parts, laid end to end along the dimension named above; an argument that names none is the same for every part. Nothing has to cross between parts.
Inputs may be any that keep to these rules, and one draw needn't show every extreme that they name: `chosen_specialist`: each row names 2 different experts. Over the whole batch no expert is named by more than 96 rows, and in every draw some expert is named by exactly 96 rows.
All inputs are finite; a program needn't handle non-finite values.
Results may differ from a plain program's by a relative error of at most 0.014.
Values may be sent and summed in bfloat16 or wider, within the bound.
A program may use at most 128 MiB of HBM per device.

v0:
```python
import jax
import jax.numpy as jnp
from jax import lax
from jax.sharding import PartitionSpec as P

LANE_WIDTH = 64
FF_E = 7168
RMS_EPS = 1e-06
GROUP_EPS = 0.00064
HIGHEST = lax.Precision.HIGHEST


def rms_norm(values, norm_gain):
    mean_sq = jnp.mean(values * values, axis=-1, keepdims=True)
    return values * lax.rsqrt(mean_sq + RMS_EPS) * norm_gain


def widen(rounded):
    return lax.optimization_barrier(rounded).astype(jnp.float32)


def evolve_memory(
    memory_arrays,
    receiver_lanes,
    address_lanes,
    content_lanes,
    forget_lanes,
    learning_lanes,
    lane_rescale,
    instant_reward,
):
    unit_key = address_lanes * lax.rsqrt(
        jnp.sum(address_lanes * address_lanes, axis=-1, keepdims=True) + 1.0
    )
    stepped_address = address_lanes * learning_lanes
    removal = jnp.einsum("bhvk,bhk->bhv", memory_arrays, unit_key, precision=HIGHEST)
    memory_after = (
        memory_arrays * forget_lanes[:, :, None, :]
        - removal[..., None] * (unit_key * learning_lanes)[:, :, None, :]
        + content_lanes[..., None] * stepped_address[:, :, None, :]
    )
    memory_retrieval = jnp.einsum("bhvk,bhk->bhv", memory_after, receiver_lanes, precision=HIGHEST)
    centred = memory_retrieval - jnp.mean(memory_retrieval, axis=-1, keepdims=True)
    unit_address = centred * lax.rsqrt(
        jnp.mean(centred * centred, axis=-1, keepdims=True) + GROUP_EPS
    )
    instant_extra = (
        jnp.sum(receiver_lanes * stepped_address * instant_reward, axis=-1, keepdims=True)
        * content_lanes
    )
    return (memory_after, unit_address * lane_rescale + instant_extra)


def swiglu(rows_in, gate_w, up_w):
    gate_val = jnp.dot(rows_in, gate_w, preferred_element_type=jnp.float32)
    up_val = jnp.dot(rows_in, up_w, preferred_element_type=jnp.float32)
    return (jax.nn.silu(gate_val) * up_val).astype(jnp.bfloat16)


def body(
    fresh_inputs,
    memory_arrays,
    chosen_specialist,
    chosen_coefficient,
    first_rescale,
    second_rescale,
    receiver_projector,
    address_projector,
    content_projector,
    final_projector,
    forget_narrowing,
    forget_widening,
    forget_bias,
    learning_narrowing,
    learning_widening,
    learning_bias,
    lane_scaling,
    instant_reward,
    specialist_switch,
    specialist_expand,
    specialist_contract,
    common_activator,
    common_expand,
    common_contract,
    common_switch,
):
    own_rows = fresh_inputs.shape[0]
    model_width = fresh_inputs.shape[1]
    tp_count = lax.axis_size("tp")
    tp_rank = lax.axis_index("tp")
    half_width = model_width // tp_count
    head_count = half_width // LANE_WIDTH
    residual = fresh_inputs.astype(jnp.float32)
    normed = rms_norm(residual, first_rescale).astype(jnp.bfloat16)
    normed_half = lax.dynamic_slice_in_dim(normed, tp_rank * half_width, half_width, 1)
    local_weights = jnp.stack((receiver_projector, address_projector, content_projector), axis=1)
    projected_rows = jnp.einsum(
        "rd,dkc->rkc",
        lax.all_gather(normed_half, "ep", axis=0, tiled=True),
        local_weights,
        preferred_element_type=jnp.float32,
    ).astype(jnp.bfloat16)
    partial_value = lax.all_to_all(projected_rows, "ep", split_axis=0, concat_axis=2, tiled=True)
    projected = lax.psum(widen(partial_value).astype(jnp.bfloat16), "tp")
    mine = lax.dynamic_slice_in_dim(projected, tp_rank * half_width, half_width, 2)

    def divide_lanes(channels):
        return channels.astype(jnp.float32).reshape(own_rows, head_count, LANE_WIDTH)

    decay_mid = jnp.tanh(
        jnp.dot(normed, forget_narrowing, preferred_element_type=jnp.float32)
    ).astype(jnp.bfloat16)
    decay_pre = forget_bias + jnp.dot(
        decay_mid, forget_widening, preferred_element_type=jnp.float32
    )
    decay_vals = jnp.exp(-jnp.exp(-jax.nn.softplus(-decay_pre) - 0.5))
    rate_mid = jnp.dot(normed, learning_narrowing, preferred_element_type=jnp.float32).astype(
        jnp.bfloat16
    )
    rate_vals = jax.nn.sigmoid(
        learning_bias + jnp.dot(rate_mid, learning_widening, preferred_element_type=jnp.float32)
    )
    memory_after, memory_retrieval = evolve_memory(
        memory_arrays,
        divide_lanes(mine[:, 0]),
        divide_lanes(mine[:, 1]),
        divide_lanes(mine[:, 2]),
        divide_lanes(decay_vals),
        divide_lanes(rate_vals),
        lane_scaling.reshape(head_count, LANE_WIDTH),
        instant_reward,
    )
    attended = memory_retrieval.reshape(own_rows, half_width).astype(jnp.bfloat16)
    done_rows = jnp.dot(
        lax.all_gather(attended, "ep", axis=0, tiled=True),
        final_projector,
        preferred_element_type=jnp.float32,
    ).astype(jnp.bfloat16)
    out_part = lax.all_to_all(done_rows, "ep", split_axis=0, concat_axis=1, tiled=True)
    mixed_out = lax.psum(widen(out_part).astype(jnp.bfloat16), "tp")
    residual = residual + mixed_out.astype(jnp.float32)
    ffn_in = rms_norm(residual, second_rescale).astype(jnp.bfloat16)
    all_in, all_weight, all_ids = (
        lax.all_gather(ffn_in, "ep", axis=0, tiled=True),
        lax.all_gather(chosen_coefficient, "ep", axis=0, tiled=True),
        lax.all_gather(chosen_specialist, "ep", axis=0, tiled=True),
    )
    column_count = specialist_switch.shape[1]
    flat_rank = lax.axis_index("ep") * tp_count + tp_rank
    expert = flat_rank * column_count // FF_E
    expert_share = jnp.sum(
        jnp.where(all_ids == expert, all_weight.astype(jnp.float32), 0.0), axis=1
    )
    hidden = swiglu(all_in, specialist_switch, specialist_expand)
    shared_hidden = swiglu(all_in, common_activator, common_expand)
    branch_scale = jax.nn.sigmoid(
        jnp.dot(all_in, common_switch, preferred_element_type=jnp.float32)
    )
    rows_mine = own_rows // tp_count
    expert_term = expert_share[:, None] * jnp.dot(
        hidden, specialist_contract, preferred_element_type=jnp.float32
    )
    routed = lax.psum_scatter(
        expert_term
        + branch_scale[:, None]
        * jnp.dot(shared_hidden, common_contract, preferred_element_type=jnp.float32),
        ("ep", "tp"),
        scatter_dimension=0,
        tiled=True,
    )
    own_residual = lax.dynamic_slice_in_dim(residual, tp_rank * rows_mine, rows_mine, 0)
    return ((own_residual + routed).astype(jnp.bfloat16), memory_after)


def solution(mesh):
    placed = (
        P(("grp", "ep"), None),
        P(("grp", "ep"), "tp", None, None),
        P(("grp", "ep"), None),
        P(("grp", "ep"), None),
        P(),
        P(),
        P("tp", "ep"),
        P("tp", "ep"),
        P("tp", "ep"),
        P("tp", "ep"),
        P(),
        P(None, "tp"),
        P("tp"),
        P(),
        P(None, "tp"),
        P("tp"),
        P("tp"),
        P("tp", None),
        P(None, ("ep", "tp")),
        P(None, ("ep", "tp")),
        P(("ep", "tp"), None),
        P(None, ("ep", "tp")),
        P(None, ("ep", "tp")),
        P(("ep", "tp"), None),
        P(),
    )
    return jax.shard_map(
        body,
        mesh=mesh,
        in_specs=placed,
        out_specs=(P(("grp", "ep", "tp"), None), P(("grp", "ep"), "tp", None, None)),
        check_vma=False,
    )
```

profile of v0, /device:TPU:0, one launch (start us, length us, event | category | flops | bytes accessed | tf_op | source)
XLA Modules:
  0.0 324.2 jit_solution(6716720031161532944)
XLA Ops:
  7.2 0.0 copy-start
  7.2 0.0 copy-start.6
  7.2 0.0 copy-start.7
  7.2 0.0 copy-start.10
  7.2 0.0 copy-start.11
  7.2 1.1 fusion.33
  8.3 0.9 fusion.35
  9.3 32.6 %all_gather.15 = bf16[128,1024]{1,0:T(8,128)(2,1)S(1)} all-gather(bf16[16,1024]{1,0:T(8,128)(2,1)S(1)} %constant_dynamic-slice_fusion.1), channel_id=1, replica_groups=mesh['grp'=2,'ep'=8,'tp'=2] {'ep'}, dimensions={0}, use_global_device_ids=true | all-gather | bytes 294912 | tf_op jit(solution)/shard_map/all_gather | solution.py:99
  41.8 1.7 fusion.9
  43.6 0.9 copy.30
  44.5 5.5 %all-to-all-start = ((bf16[128,3,256]{2,1,0:T(4,128)(2,1)}), bf16[128,3,256]{2,1,0:T(4,128)(2,1)S(1)}, u32[]{:S(2)}, u32[]{:S(2)}) async-start(bf16[128,3,256]{2,1,0:T(4,128)(2,1)} %copy.30), calls=%async_computation | async-start | bytes 524288 | tf_op jit(solution)/shard_map/all_to_all | solution.py:103
  50.0 0.0 all-reduce.3.cloned.1.call-start
  50.0 1.4 fusion.19
  51.4 0.1 reshape.102
  51.5 6.7 %all-to-all-done = bf16[128,3,256]{2,1,0:T(4,128)(2,1)S(1)} async-done(((bf16[128,3,256]{2,1,0:T(4,128)(2,1)}), bf16[128,3,256]{2,1,0:T(4,128)(2,1)S(1)}, u32[]{:S(2)}, u32[]{:S(2)}) %all-to-all-start) | async-done | bytes 196640 | tf_op jit(solution)/shard_map/all_to_all | solution.py:103
  58.2 0.1 copy.39
  58.3 0.8 all_to_all.30
  59.1 0.0 all-reduce.3.cloned.1.call-update
  59.2 0.4 fusion.42
  59.6 0.1 mul.207
  59.7 0.1 mul.225
  59.7 15.9 %all-reduce.3.cloned.1.call-done = bf16[16,3,2048]{2,0,1:T(8,128)(2,1)} async-done(((bf16[16,3,2048]{2,0,1:T(8,128)(2,1)}), bf16[16,3,2048]{2,0,1:T(8,128)(2,1)}) %all-reduce.3.cloned.1.call-update) | async-done | bytes 196624 | tf_op jit(solution)/shard_map/psum | solution.py:104
  75.7 0.8 constant_dynamic-slice_fusion
  76.5 0.1 reshape.124
  76.6 0.1 reshape.103
  76.7 0.1 reshape.104
  76.8 0.1 multiply_reduce_fusion.2
  76.9 0.1 reshape.105
  77.0 0.1 fusion.48
  77.1 15.4 %fusion.49 = f32[16,16,1,64]{3,2,1,0:T(1,128)S(1)} fusion(f32[16,16,64,1]{2,3,1,0:T(1,128)S(1)} %bitcast.75, f32[16,16,64,64]{3,2,1,0:T(8,128)} %param.26), kind=kOutput, calls=%fused_computation.80 | convolution fusion | flops 12582912 | bytes 4325376 | tf_op jit(solution)/shard_map/bhvk,bhk->bhv/dot_general | solution.py:36
  92.5 8.6 %multiply_add_fusion = f32[16,16,64,64]{3,2,1,0:T(8,128)S(1)} fusion(f32[16,16,64,64]{3,2,1,0:T(8,128)} %param.26, f32[16,16,64]{2,1,0:T(8,128)S(1)} %get-tuple-element.4, f32[16,16,64]{2,1,0:T(8,128)S(1)} %reshape.105, f32[16,16,64]{2,1,0:T(8,128)S(1)} %get-tuple-element.2, f32[16,16,64]{2,1,0:T(8,128)S(1)} %bitcast.74, f32[16,16,64]{2,1,0:T(8,128)S(1)} %mul.207), kind=kLoop, calls=%fused_computation.1 | loop fusion | flops 5242880 | bytes 8716288 | tf_op jit(solution)/shard_map/add | solution.py:38
  101.1 0.0 copy-start.1
  101.1 3.4 %copy-done.1 = f32[16,16,64,64]{3,2,1,0:T(8,128)} copy-done((f32[16,16,64,64]{3,2,1,0:T(8,128)}, f32[16,16,64,64]{3,2,1,0:T(8,128)S(1)}, u32[]{:S(2)}) %copy-start.1) | copy-done | bytes 4194328
  104.5 0.0 copy-start.12
  104.5 0.0 copy-start.4
  104.5 0.0 copy-start.9
  104.6 6.6 %fusion.50 = f32[16,16,1,64]{3,2,1,0:T(1,128)S(1)} fusion(f32[16,16,64,64]{3,2,1,0:T(8,128)S(1)} %multiply_add_fusion, bf16[16,16,64,1]{2,3,1,0:T(2,128)(2,1)S(1)} %reshape.124), kind=kOutput, calls=%fused_computation.81 | convolution fusion | flops 12582912 | bytes 4292608 | tf_op jit(solution)/shard_map/bhvk,bhk->bhv/dot_general | solution.py:42
  111.2 0.1 reduce_sum.65
  111.3 0.2 multiply_reduce_fusion.1
  111.5 0.5 fusion.15
  112.0 0.1 convert_element_type.98
  112.2 31.1 %all_gather.16 = bf16[128,1024]{1,0:T(8,128)(2,1)S(1)} all-gather(bf16[16,1024]{1,0:T(8,128)(2,1)S(1)} %convert_element_type.98), channel_id=1, replica_groups=mesh['grp'=2,'ep'=8,'tp'=2] {'ep'}, dimensions={0}, use_global_device_ids=true | all-gather | bytes 294912 | tf_op jit(solution)/shard_map/all_gather | solution.py:135
  143.3 0.8 convolution_convert_fusion
  144.1 5.4 %all-to-all-start.1 = ((bf16[8,16,256]{2,1,0:T(8,128)(2,1)}), bf16[8,16,256]{2,1,0:T(8,128)(2,1)S(1)}, u32[]{:S(2)}, u32[]{:S(2)}) async-start(bf16[8,16,256]{2,1,0:T(8,128)(2,1)} %bitcast.12), calls=%async_computation.1 | async-start | bytes 131072 | tf_op jit(solution)/shard_map/all_to_all | solution.py:139
  149.6 0.0 all-reduce.5.cloned.1.call-start
  149.6 20.9 %all-gather.1 = bf16[8,16,2]{1,2,0:T(2,128)(2,1)S(1)} all-gather(bf16[1,16,2]{1,2,0:T(2,128)(2,1)S(1)} %bitcast.79), channel_id=1, replica_groups=mesh['grp'=2,'ep'=8,'tp'=2] {'ep'}, dimensions={0}, use_global_device_ids=true | all-gather | bytes 576 | tf_op jit(solution)/shard_map/all_gather | solution.py:145
  170.6 16.5 %all-gather = s32[8,16,2]{1,2,0:T(2,128)S(1)} all-gather(s32[1,16,2]{1,2,0:T(2,128)S(1)} %bitcast.78), channel_id=1, replica_groups=mesh['grp'=2,'ep'=8,'tp'=2] {'ep'}, dimensions={0}, use_global_device_ids=true | all-gather | bytes 1152 | tf_op jit(solution)/shard_map/all_gather | solution.py:146
  187.0 0.0 all-to-all-done.1
  187.0 0.6 copy.37
  187.6 0.0 all-reduce.5.cloned.1.call-update
  187.7 0.0 reduce-scatter.2.cloned.1.call-start
  187.7 0.1 reshape.115
  187.8 16.4 %all-reduce.5.cloned.1.call-done = bf16[16,2048]{1,0:T(8,128)(2,1)} async-done(((bf16[16,2048]{1,0:T(8,128)(2,1)}), bf16[16,2048]{1,0:T(8,128)(2,1)}) %all-reduce.5.cloned.1.call-update) | async-done | bytes 65552 | tf_op jit(solution)/shard_map/psum | solution.py:140
  204.2 1.0 convert_add_fusion
  205.2 0.9 multiply_convert_fusion
  206.1 31.8 %all_gather.19 = bf16[128,2048]{1,0:T(8,128)(2,1)S(1)} all-gather(bf16[16,2048]{1,0:T(8,128)(2,1)S(1)} %multiply_convert_fusion), channel_id=1, replica_groups=mesh['grp'=2,'ep'=8,'tp'=2] {'ep'}, dimensions={0}, use_global_device_ids=true | all-gather | bytes 589824 | tf_op jit(solution)/shard_map/all_gather | solution.py:144
  237.9 5.3 %fusion.51 = f32[128,1792]{1,0:T(8,128)} fusion(bf16[128,2048]{1,0:T(8,128)(2,1)S(1)} %all_gather.19, bf16[2048,1792]{1,0:T(8,128)(2,1)} %param.43), kind=kOutput, calls=%fused_computation.82 | convolution fusion | flops 939524096 | bytes 8781824 | tf_op jit(solution)/shard_map/dot_general | solution.py:55
  243.2 1.2 fusion.52
  244.4 0.2 fusion.25
  244.7 9.1 %convolution_multiply_fusion.1 = f32[128,2048]{1,0:T(8,128)} fusion(bf16[1792,2048]{1,0:T(8,128)(2,1)} %param.45, bf16[128,2048]{1,0:T(8,128)(2,1)S(1)} %all_gather.19, bf16[2048,1792]{1,0:T(8,128)(2,1)} %param.44, f32[128,1792]{1,0:T(8,128)} %fusion.51, f32[128]{0:T(128)S(1)} %reshape.115), kind=kOutput, calls=%fused_computation.3 | convolution fusion | flops 1880686592 | bytes 17170944 | tf_op jit(solution)/shard_map/dot_general | solution.py:160
  253.7 3.8 %fusion.1 = f32[128,2048]{1,0:T(8,128)} fusion(f32[128,2048]{1,0:T(8,128)} %convolution_multiply_fusion.1, bf16[352,2048]{1,0:T(8,128)(2,1)S(1)} %copy-done, bf16[128,2048]{1,0:T(8,128)(2,1)S(1)} %all_gather.19, bf16[2048,352]{0,1:T(8,128)(2,1)S(1)} %copy-done.3, f32[128]{0:T(128)S(1)} %fusion.25, f32[128,352]{0,1:T(8,128)} %fusion.52), kind=kOutput, calls=%fused_computation.5 | convolution fusion | flops 369893376 | bytes 5685760 | tf_op jit(solution)/shard_map/dot_general | solution.py:166
  257.5 0.0 reduce-scatter.2.cloned.1.call-update
  257.6 58.6 %reduce-scatter.2.cloned.1.call-done = f32[8,2048]{1,0:T(8,128)} async-done(((f32[128,2048]{1,0:T(8,128)}), f32[8,2048]{1,0:T(8,128)}) %reduce-scatter.2.cloned.1.call-update) | async-done | bytes 65552 | tf_op jit(solution)/shard_map/reduce_scatter | solution.py:163
  316.2 1.5 add_convert_fusion
  (28 shorter events, 0.1 us)
Async XLA Ops:
  7.2 246.6 %copy-start = (bf16[352,2048]{1,0:T(8,128)(2,1)S(1)}, bf16[352,2048]{1,0:T(8,128)(2,1)}, u32[]{:S(2)}) copy-start(bf16[352,2048]{1,0:T(8,128)(2,1)} %param.48) | copy-start | bytes 4325380
  7.2 52.0 %copy-start.6 = (bf16[2048,64]{0,1:T(8,128)(2,1)S(1)}, bf16[2048,64]{0,1:T(8,128)(2,1)}, u32[]{:S(2)}) copy-start(bf16[2048,64]{0,1:T(8,128)(2,1)} %param.35) | copy-start | bytes 786436
  7.2 52.0 %copy-start.7 = (bf16[64,1024]{1,0:T(8,128)(2,1)S(1)}, bf16[64,1024]{1,0:T(8,128)(2,1)}, u32[]{:S(2)}) copy-start(bf16[64,1024]{1,0:T(8,128)(2,1)} %param.36) | copy-start | bytes 393220
  7.2 52.0 %copy-start.10 = (f32[1024]{0:T(1024)S(1)}, f32[1024]{0:T(1024)}, u32[]{:S(2)}) copy-start(f32[1024]{0:T(1024)} %param.37) | copy-start | bytes 12292
  7.2 52.5 %copy-start.11 = (f32[1024]{0:T(1024)S(1)}, f32[1024]{0:T(1024)}, u32[]{:S(2)}) copy-start(f32[1024]{0:T(1024)} %param.41) | copy-start | bytes 12292
  44.5 13.7 %all-to-all-start = ((bf16[128,3,256]{2,1,0:T(4,128)(2,1)}), bf16[128,3,256]{2,1,0:T(4,128)(2,1)S(1)}, u32[]{:S(2)}, u32[]{:S(2)}) async-start(bf16[128,3,256]{2,1,0:T(4,128)(2,1)} %copy.30), calls=%async_computation | async-start | bytes 524288 | tf_op jit(solution)/shard_map/all_to_all | solution.py:103
  50.0 25.7 %all-reduce.3.cloned.1.call-start = ((), (), s32[]{:S(2)}) async-start(), calls=%async_computation.3 | async-start | bytes 393216 | tf_op jit(solution)/shard_map/psum | solution.py:104
  101.1 3.4 %copy-start.1 = (f32[16,16,64,64]{3,2,1,0:T(8,128)}, f32[16,16,64,64]{3,2,1,0:T(8,128)S(1)}, u32[]{:S(2)}) copy-start(f32[16,16,64,64]{3,2,1,0:T(8,128)S(1)} %multiply_add_fusion) | copy-start | bytes 12582916
  104.5 7.0 %copy-start.8 = (f32[16,64]{1,0:T(8,128)S(1)}, f32[16,64]{1,0:T(8,128)}, u32[]{:S(2)}) copy-start(f32[16,64]{1,0:T(8,128)} %param.42) | copy-start | bytes 12292
  104.5 38.8 %copy-start.5 = (bf16[1024,256]{1,0:T(8,128)(2,1)S(1)}, bf16[1024,256]{1,0:T(8,128)(2,1)}, u32[]{:S(2)}) copy-start(bf16[1024,256]{1,0:T(8,128)(2,1)} %param.34) | copy-start | bytes 1572868
  104.5 45.1 %copy-start.14 = (bf16[16,2]{0,1:T(2,128)(2,1)S(1)}, bf16[16,2]{0,1:T(2,128)(2,1)}, u32[]{:S(2)}) copy-start(bf16[16,2]{0,1:T(2,128)(2,1)} %param.28) | copy-start | bytes 196
  104.5 66.0 %copy-start.13 = (s32[16,2]{0,1:T(2,128)S(1)}, s32[16,2]{0,1:T(2,128)}, u32[]{:S(2)}) copy-start(s32[16,2]{0,1:T(2,128)} %param.27) | copy-start | bytes 388
  104.5 83.3 %copy-start.12 = (bf16[2048]{0:T(1024)(128)(2,1)S(1)}, bf16[2048]{0:T(1024)(128)(2,1)}, u32[]{:S(2)}) copy-start(bf16[2048]{0:T(1024)(128)(2,1)} %param.49) | copy-start | bytes 12292
  104.5 99.7 %copy-start.4 = (bf16[16,2048]{1,0:T(8,128)(2,1)S(1)}, bf16[16,2048]{1,0:T(8,128)(2,1)}, u32[]{:S(2)}) copy-start(bf16[16,2048]{1,0:T(8,128)(2,1)} %param.25) | copy-start | bytes 196612
  104.5 100.7 %copy-start.9 = (f32[2048]{0:T(1024)S(1)}, f32[2048]{0:T(1024)}, u32[]{:S(2)}) copy-start(f32[2048]{0:T(1024)} %param.30) | copy-start | bytes 24580
  144.1 42.9 %all-to-all-start.1 = ((bf16[8,16,256]{2,1,0:T(8,128)(2,1)}), bf16[8,16,256]{2,1,0:T(8,128)(2,1)S(1)}, u32[]{:S(2)}, u32[]{:S(2)}) async-start(bf16[8,16,256]{2,1,0:T(8,128)(2,1)} %bitcast.12), calls=%async_computation.1 | async-start | bytes 131072 | tf_op jit(solution)/shard_map/all_to_all | solution.py:139
  149.6 54.7 %all-reduce.5.cloned.1.call-start = ((), (), s32[]{:S(2)}) async-start(), calls=%async_computation.4 | async-start | bytes 131072 | tf_op jit(solution)/shard_map/psum | solution.py:140
  187.7 128.5 %reduce-scatter.2.cloned.1.call-start = ((), (), s32[]{:S(2)}) async-start(), calls=%async_computation.5 | async-start | bytes 1114112 | tf_op jit(solution)/shard_map/reduce_scatter | solution.py:163
  237.9 5.3 %copy-start.2 = (bf16[2048,352]{0,1:T(8,128)(2,1)S(1)}, bf16[2048,352]{0,1:T(8,128)(2,1)}, u32[]{:S(2)}) copy-start(bf16[2048,352]{0,1:T(8,128)(2,1)} %param.46) | copy-start | bytes 4325380
  244.7 9.1 %copy-start.3 = (bf16[2048,352]{0,1:T(8,128)(2,1)S(1)}, bf16[2048,352]{0,1:T(8,128)(2,1)}, u32[]{:S(2)}) copy-start(bf16[2048,352]{0,1:T(8,128)(2,1)} %param.47) | copy-start | bytes 4325380
Sparse Core Ops, SparseCore 0:
  59.3 16.3 all-reduce.2
  187.8 16.3 all-reduce.4
  257.7 58.4 reduce-scatter.1
where the time goes:
time: 325 us; the launch traced here: 324 us
  blocking collectives  133 us (41%)
  waiting for transfers between devices  97.7 us (30%)
  matrix products  46 us (14%)
  other arithmetic  15.8 us (5%)
  between operations  14.1 us (4%)
  starting transfers between devices  11.1 us (3%)
  local copies, waits for them, and re-layouts  6.74 us (2%)
    reduce_scatter x1, waiting for transfers between devices, body(): lax.psum_scatter(expert_term + branch_scale[:, None] * jnp.dot(shared_hid...  58.6 us
    all_gather x1, blocking collectives, body(): lax.all_gather(normed_half, 'ep', axis=0, tiled=True)  32.6 us
    all_gather x1, blocking collectives, body(): lax.all_gather(ffn_in, 'ep', axis=0, tiled=True)  31.8 us
    all_gather x1, blocking collectives, body(): lax.all_gather(attended, 'ep', axis=0, tiled=True)  31.1 us
    all_gather x1, blocking collectives, body(): lax.all_gather(chosen_coefficient, 'ep', axis=0, tiled=True)  20.9 us
    all_gather x1, blocking collectives, body(): lax.all_gather(chosen_specialist, 'ep', axis=0, tiled=True)  16.5 us
    psum x1, waiting for transfers between devices, body(): mixed_out = lax.psum(widen(out_part).astype(jnp.bfloat16), 'tp')  16.4 us
    psum x1, waiting for transfers between devices, body(): projected = lax.psum(widen(partial_value).astype(jnp.bfloat16), 'tp')  15.9 us
  transfers between devices with their start and end apart: 5, of which 4 were waited for; matrix products, arithmetic and copies ran while one was open for 1% of the time, Pallas kernels for 0%

commit v1 on v0

--- a/solution.py
+++ b/solution.py
@@ -137,7 +137,9 @@
         preferred_element_type=jnp.float32,
     ).astype(jnp.bfloat16)
     out_part = lax.all_to_all(done_rows, "ep", split_axis=0, concat_axis=1, tiled=True)
-    mixed_out = lax.psum(widen(out_part).astype(jnp.bfloat16), "tp")
+    own = widen(out_part).astype(jnp.bfloat16)
+    parts = lax.all_gather(own, "tp")
+    mixed_out = jnp.sum(parts, axis=0)
     residual = residual + mixed_out.astype(jnp.float32)
     ffn_in = rms_norm(residual, second_rescale).astype(jnp.bfloat16)
     all_in, all_weight, all_ids = (

time: 325 us -> 306 us (0.942)
  waiting for transfers between devices: 97.7 us -> 79.4 us
    psum x1 -> x0, waiting for transfers between devices: 16.4 us -> none  [body(): mixed_out = lax.psum(widen(out_part).astype(jnp.bfloat16), 'tp')]
  transfers between devices with their start and end apart: 5 -> 4, of which waited for: 4 -> 3; matrix products, arithmetic and copies ran while one was open for 1% -> 1% of each run, Pallas kernels for 0% -> 0%
where the time goes in v1:
time: 306 us; the launch traced here: 305 us
  blocking collectives  134 us (44%)
  waiting for transfers between devices  79.4 us (26%)
  matrix products  46 us (15%)
  between operations  14.4 us (5%)
  other arithmetic  14.2 us (5%)
  starting transfers between devices  11 us (4%)
  local copies, waits for them, and re-layouts  6.13 us (2%)
    reduce_scatter x1, waiting for transfers between devices, body(): lax.psum_scatter(expert_term + branch_scale[:, None] * jnp.dot(shared_hid...  56.8 us
    all_gather x1, blocking collectives, body(): lax.all_gather(normed_half, 'ep', axis=0, tiled=True)  32.6 us
    all_gather x1, blocking collectives, body(): lax.all_gather(ffn_in, 'ep', axis=0, tiled=True)  31.3 us
    all_gather x1, blocking collectives, body(): lax.all_gather(attended, 'ep', axis=0, tiled=True)  31.1 us
    all_gather x1, blocking collectives, body(): lax.all_gather(chosen_coefficient, 'ep', axis=0, tiled=True)  20.9 us
    all_gather x1, blocking collectives, body(): lax.all_gather(chosen_specialist, 'ep', axis=0, tiled=True)  16.5 us
    psum x1, waiting for transfers between devices, body(): projected = lax.psum(widen(partial_value).astype(jnp.bfloat16), 'tp')  15.9 us
    dot_general x1, matrix products, evolve_memory(): jnp.einsum('bhvk,bhk->bhv', memory_arrays, unit_key, precision=HIGHEST)  15.4 us
  transfers between devices with their start and end apart: 4, of which 3 were waited for; matrix products, arithmetic and copies ran while one was open for 1% of the time, Pallas kernels for 0%

profile of v1, /device:TPU:0, one launch (start us, length us, event | category | flops | bytes accessed | tf_op | source)
XLA Modules:
  0.0 305.4 jit_solution(11259267874771029587)
XLA Ops:
  7.2 0.0 copy-start
  7.2 0.0 copy-start.6
  7.2 0.0 copy-start.7
  7.2 0.0 copy-start.10
  7.2 0.0 copy-start.11
  7.2 1.1 fusion.33
  8.3 0.9 fusion.35
  9.3 32.6 %all_gather.21 = bf16[128,1024]{1,0:T(8,128)(2,1)S(1)} all-gather(bf16[16,1024]{1,0:T(8,128)(2,1)S(1)} %constant_dynamic-slice_fusion.1), channel_id=1, replica_groups=mesh['grp'=2,'ep'=8,'tp'=2] {'ep'}, dimensions={0}, use_global_device_ids=true | all-gather | bytes 294912 | tf_op jit(solution)/shard_map/all_gather | solution.py:99
  41.8 1.7 fusion.9
  43.6 0.9 copy.29
  44.5 5.5 %all-to-all-start = ((bf16[128,3,256]{2,1,0:T(4,128)(2,1)}), bf16[128,3,256]{2,1,0:T(4,128)(2,1)S(1)}, u32[]{:S(2)}, u32[]{:S(2)}) async-start(bf16[128,3,256]{2,1,0:T(4,128)(2,1)} %copy.29), calls=%async_computation | async-start | bytes 524288 | tf_op jit(solution)/shard_map/all_to_all | solution.py:103
  50.0 0.0 all-reduce.2.cloned.1.call-start
  50.0 1.4 fusion.19
  51.4 0.1 reshape.102
  51.5 6.7 %all-to-all-done = bf16[128,3,256]{2,1,0:T(4,128)(2,1)S(1)} async-done(((bf16[128,3,256]{2,1,0:T(4,128)(2,1)}), bf16[128,3,256]{2,1,0:T(4,128)(2,1)S(1)}, u32[]{:S(2)}, u32[]{:S(2)}) %all-to-all-start) | async-done | bytes 196640 | tf_op jit(solution)/shard_map/all_to_all | solution.py:103
  58.2 0.1 copy.38
  58.3 0.8 all_to_all.30
  59.1 0.0 all-reduce.2.cloned.1.call-update
  59.1 0.0 copy-done.6
  59.2 0.0 copy-done.7
  59.2 0.0 copy-done.10
  59.2 0.4 fusion.42
  59.6 0.1 mul.207
  59.7 0.1 mul.225
  59.7 15.9 %all-reduce.2.cloned.1.call-done = bf16[16,3,2048]{2,0,1:T(8,128)(2,1)} async-done(((bf16[16,3,2048]{2,0,1:T(8,128)(2,1)}), bf16[16,3,2048]{2,0,1:T(8,128)(2,1)}) %all-reduce.2.cloned.1.call-update) | async-done | bytes 196624 | tf_op jit(solution)/shard_map/psum | solution.py:104
  75.7 0.8 constant_dynamic-slice_fusion
  76.5 0.1 reshape.125
  76.6 0.1 reshape.103
  76.7 0.1 reshape.104
  76.8 0.1 multiply_reduce_fusion.2
  76.9 0.1 reshape.105
  77.0 0.1 fusion.48
  77.1 15.4 %fusion.49 = f32[16,16,1,64]{3,2,1,0:T(1,128)S(1)} fusion(f32[16,16,64,1]{2,3,1,0:T(1,128)S(1)} %bitcast.76, f32[16,16,64,64]{3,2,1,0:T(8,128)} %param.26), kind=kOutput, calls=%fused_computation.80 | convolution fusion | flops 12582912 | bytes 4325376 | tf_op jit(solution)/shard_map/bhvk,bhk->bhv/dot_general | solution.py:36
  92.5 8.6 %multiply_add_fusion = f32[16,16,64,64]{3,2,1,0:T(8,128)S(1)} fusion(f32[16,16,64,64]{3,2,1,0:T(8,128)} %param.26, f32[16,16,64]{2,1,0:T(8,128)S(1)} %get-tuple-element.4, f32[16,16,64]{2,1,0:T(8,128)S(1)} %reshape.105, f32[16,16,64]{2,1,0:T(8,128)S(1)} %get-tuple-element.2, f32[16,16,64]{2,1,0:T(8,128)S(1)} %bitcast.75, f32[16,16,64]{2,1,0:T(8,128)S(1)} %mul.207), kind=kLoop, calls=%fused_computation.1 | loop fusion | flops 5242880 | bytes 8716288 | tf_op jit(solution)/shard_map/add | solution.py:38
  101.1 0.0 copy-start.1
  101.1 3.4 %copy-done.1 = f32[16,16,64,64]{3,2,1,0:T(8,128)} copy-done((f32[16,16,64,64]{3,2,1,0:T(8,128)}, f32[16,16,64,64]{3,2,1,0:T(8,128)S(1)}, u32[]{:S(2)}) %copy-start.1) | copy-done | bytes 4194328
  104.5 0.0 copy-start.12
  104.5 0.0 copy-start.4
  104.5 0.0 copy-start.9
  104.6 6.6 %fusion.50 = f32[16,16,1,64]{3,2,1,0:T(1,128)S(1)} fusion(f32[16,16,64,64]{3,2,1,0:T(8,128)S(1)} %multiply_add_fusion, bf16[16,16,64,1]{2,3,1,0:T(2,128)(2,1)S(1)} %reshape.125), kind=kOutput, calls=%fused_computation.81 | convolution fusion | flops 12582912 | bytes 4292608 | tf_op jit(solution)/shard_map/bhvk,bhk->bhv/dot_general | solution.py:42
  111.2 0.1 reduce_sum.77
  111.3 0.2 multiply_reduce_fusion.1
  111.5 0.5 fusion.15
  112.0 0.1 convert_element_type.100
  112.2 31.1 %all_gather.22 = bf16[128,1024]{1,0:T(8,128)(2,1)S(1)} all-gather(bf16[16,1024]{1,0:T(8,128)(2,1)S(1)} %convert_element_type.100), channel_id=1, replica_groups=mesh['grp'=2,'ep'=8,'tp'=2] {'ep'}, dimensions={0}, use_global_device_ids=true | all-gather | bytes 294912 | tf_op jit(solution)/shard_map/all_gather | solution.py:135
  143.3 0.9 convolution_convert_fusion
  144.1 5.4 %all-to-all-start.1 = ((bf16[8,16,256]{2,1,0:T(8,128)(2,1)}), bf16[8,16,256]{2,1,0:T(8,128)(2,1)S(1)}, u32[]{:S(2)}, u32[]{:S(2)}) async-start(bf16[8,16,256]{2,1,0:T(8,128)(2,1)} %bitcast.12), calls=%async_computation.1 | async-start | bytes 131072 | tf_op jit(solution)/shard_map/all_to_all | solution.py:139
  149.6 0.0 reduce-scatter.2.cloned.1.call-start
  149.6 20.9 %all-gather.2 = bf16[8,16,2]{1,2,0:T(2,128)(2,1)S(1)} all-gather(bf16[1,16,2]{1,2,0:T(2,128)(2,1)S(1)} %bitcast.81), channel_id=1, replica_groups=mesh['grp'=2,'ep'=8,'tp'=2] {'ep'}, dimensions={0}, use_global_device_ids=true | all-gather | bytes 576 | tf_op jit(solution)/shard_map/all_gather | solution.py:147
  170.6 16.5 %all-gather.1 = s32[8,16,2]{1,2,0:T(2,128)S(1)} all-gather(s32[1,16,2]{1,2,0:T(2,128)S(1)} %bitcast.80), channel_id=1, replica_groups=mesh['grp'=2,'ep'=8,'tp'=2] {'ep'}, dimensions={0}, use_global_device_ids=true | all-gather | bytes 1152 | tf_op jit(solution)/shard_map/all_gather | solution.py:148
  187.0 0.1 reshape.116
  187.1 0.0 all-to-all-done.1
  187.2 1.9 all-gather
  189.1 0.1 convert_add_fusion
  189.3 0.1 multiply_convert_fusion
  189.3 31.3 %all_gather.27 = bf16[128,2048]{1,0:T(8,128)(2,1)S(1)} all-gather(bf16[16,2048]{1,0:T(8,128)(2,1)S(1)} %multiply_convert_fusion), channel_id=1, replica_groups=mesh['grp'=2,'ep'=8,'tp'=2] {'ep'}, dimensions={0}, use_global_device_ids=true | all-gather | bytes 589824 | tf_op jit(solution)/shard_map/all_gather | solution.py:146
  220.7 5.3 %fusion.51 = f32[128,1792]{1,0:T(8,128)} fusion(bf16[128,2048]{1,0:T(8,128)(2,1)S(1)} %all_gather.27, bf16[2048,1792]{1,0:T(8,128)(2,1)} %param.43), kind=kOutput, calls=%fused_computation.82 | convolution fusion | flops 939524096 | bytes 8781824 | tf_op jit(solution)/shard_map/dot_general | solution.py:55
  226.0 1.2 fusion.52
  227.2 0.2 fusion.25
  227.4 9.1 %convolution_multiply_fusion.1 = f32[128,2048]{1,0:T(8,128)} fusion(bf16[1792,2048]{1,0:T(8,128)(2,1)} %param.45, bf16[128,2048]{1,0:T(8,128)(2,1)S(1)} %all_gather.27, bf16[2048,1792]{1,0:T(8,128)(2,1)} %param.44, f32[128,1792]{1,0:T(8,128)} %fusion.51, f32[128]{0:T(128)S(1)} %reshape.116), kind=kOutput, calls=%fused_computation.3 | convolution fusion | flops 1880686592 | bytes 17170944 | tf_op jit(solution)/shard_map/dot_general | solution.py:162
  236.5 3.8 %fusion.1 = f32[128,2048]{1,0:T(8,128)} fusion(f32[128,2048]{1,0:T(8,128)} %convolution_multiply_fusion.1, bf16[352,2048]{1,0:T(8,128)(2,1)S(1)} %copy-done, bf16[128,2048]{1,0:T(8,128)(2,1)S(1)} %all_gather.27, bf16[2048,352]{0,1:T(8,128)(2,1)S(1)} %copy-done.3, f32[128]{0:T(128)S(1)} %fusion.25, f32[128,352]{0,1:T(8,128)} %fusion.52), kind=kOutput, calls=%fused_computation.5 | convolution fusion | flops 369893376 | bytes 5685760 | tf_op jit(solution)/shard_map/dot_general | solution.py:168
  240.3 0.0 reduce-scatter.2.cloned.1.call-update
  240.3 56.8 %reduce-scatter.2.cloned.1.call-done = f32[8,2048]{1,0:T(8,128)} async-done(((f32[128,2048]{1,0:T(8,128)}), f32[8,2048]{1,0:T(8,128)}) %reduce-scatter.2.cloned.1.call-update) | async-done | bytes 65552 | tf_op jit(solution)/shard_map/reduce_scatter | solution.py:165
  297.1 1.5 add_convert_fusion
  (27 shorter events, 0.1 us)
Async XLA Ops:
  7.2 229.3 %copy-start = (bf16[352,2048]{1,0:T(8,128)(2,1)S(1)}, bf16[352,2048]{1,0:T(8,128)(2,1)}, u32[]{:S(2)}) copy-start(bf16[352,2048]{1,0:T(8,128)(2,1)} %param.48) | copy-start | bytes 4325380
  7.2 52.0 %copy-start.6 = (bf16[2048,64]{0,1:T(8,128)(2,1)S(1)}, bf16[2048,64]{0,1:T(8,128)(2,1)}, u32[]{:S(2)}) copy-start(bf16[2048,64]{0,1:T(8,128)(2,1)} %param.35) | copy-start | bytes 786436
  7.2 52.0 %copy-start.7 = (bf16[64,1024]{1,0:T(8,128)(2,1)S(1)}, bf16[64,1024]{1,0:T(8,128)(2,1)}, u32[]{:S(2)}) copy-start(bf16[64,1024]{1,0:T(8,128)(2,1)} %param.36) | copy-start | bytes 393220
  7.2 52.0 %copy-start.10 = (f32[1024]{0:T(1024)S(1)}, f32[1024]{0:T(1024)}, u32[]{:S(2)}) copy-start(f32[1024]{0:T(1024)} %param.37) | copy-start | bytes 12292
  7.2 52.5 %copy-start.11 = (f32[1024]{0:T(1024)S(1)}, f32[1024]{0:T(1024)}, u32[]{:S(2)}) copy-start(f32[1024]{0:T(1024)} %param.41) | copy-start | bytes 12292
  44.5 13.7 %all-to-all-start = ((bf16[128,3,256]{2,1,0:T(4,128)(2,1)}), bf16[128,3,256]{2,1,0:T(4,128)(2,1)S(1)}, u32[]{:S(2)}, u32[]{:S(2)}) async-start(bf16[128,3,256]{2,1,0:T(4,128)(2,1)} %copy.29), calls=%async_computation | async-start | bytes 524288 | tf_op jit(solution)/shard_map/all_to_all | solution.py:103
  50.0 25.7 %all-reduce.2.cloned.1.call-start = ((), (), s32[]{:S(2)}) async-start(), calls=%async_computation.3 | async-start | bytes 393216 | tf_op jit(solution)/shard_map/psum | solution.py:104
  101.1 3.4 %copy-start.1 = (f32[16,16,64,64]{3,2,1,0:T(8,128)}, f32[16,16,64,64]{3,2,1,0:T(8,128)S(1)}, u32[]{:S(2)}) copy-start(f32[16,16,64,64]{3,2,1,0:T(8,128)S(1)} %multiply_add_fusion) | copy-start | bytes 12582916
  104.5 7.0 %copy-start.8 = (f32[16,64]{1,0:T(8,128)S(1)}, f32[16,64]{1,0:T(8,128)}, u32[]{:S(2)}) copy-start(f32[16,64]{1,0:T(8,128)} %param.42) | copy-start | bytes 12292
  104.5 38.8 %copy-start.5 = (bf16[1024,256]{1,0:T(8,128)(2,1)S(1)}, bf16[1024,256]{1,0:T(8,128)(2,1)}, u32[]{:S(2)}) copy-start(bf16[1024,256]{1,0:T(8,128)(2,1)} %param.34) | copy-start | bytes 1572868
  104.5 45.1 %copy-start.14 = (bf16[16,2]{0,1:T(2,128)(2,1)S(1)}, bf16[16,2]{0,1:T(2,128)(2,1)}, u32[]{:S(2)}) copy-start(bf16[16,2]{0,1:T(2,128)(2,1)} %param.28) | copy-start | bytes 196
  104.5 66.0 %copy-start.13 = (s32[16,2]{0,1:T(2,128)S(1)}, s32[16,2]{0,1:T(2,128)}, u32[]{:S(2)}) copy-start(s32[16,2]{0,1:T(2,128)} %param.27) | copy-start | bytes 388
  104.5 82.6 %copy-start.12 = (bf16[2048]{0:T(1024)(128)(2,1)S(1)}, bf16[2048]{0:T(1024)(128)(2,1)}, u32[]{:S(2)}) copy-start(bf16[2048]{0:T(1024)(128)(2,1)} %param.49) | copy-start | bytes 12292
  104.5 84.6 %copy-start.4 = (bf16[16,2048]{1,0:T(8,128)(2,1)S(1)}, bf16[16,2048]{1,0:T(8,128)(2,1)}, u32[]{:S(2)}) copy-start(bf16[16,2048]{1,0:T(8,128)(2,1)} %param.25) | copy-start | bytes 196612
  104.5 84.7 %copy-start.9 = (f32[2048]{0:T(1024)S(1)}, f32[2048]{0:T(1024)}, u32[]{:S(2)}) copy-start(f32[2048]{0:T(1024)} %param.30) | copy-start | bytes 24580
  144.1 43.0 %all-to-all-start.1 = ((bf16[8,16,256]{2,1,0:T(8,128)(2,1)}), bf16[8,16,256]{2,1,0:T(8,128)(2,1)S(1)}, u32[]{:S(2)}, u32[]{:S(2)}) async-start(bf16[8,16,256]{2,1,0:T(8,128)(2,1)} %bitcast.12), calls=%async_computation.1 | async-start | bytes 131072 | tf_op jit(solution)/shard_map/all_to_all | solution.py:139
  149.6 147.5 %reduce-scatter.2.cloned.1.call-start = ((), (), s32[]{:S(2)}) async-start(), calls=%async_computation.4 | async-start | bytes 1114112 | tf_op jit(solution)/shard_map/reduce_scatter | solution.py:165
  220.7 5.3 %copy-start.2 = (bf16[2048,352]{0,1:T(8,128)(2,1)S(1)}, bf16[2048,352]{0,1:T(8,128)(2,1)}, u32[]{:S(2)}) copy-start(bf16[2048,352]{0,1:T(8,128)(2,1)} %param.46) | copy-start | bytes 4325380
  227.4 9.1 %copy-start.3 = (bf16[2048,352]{0,1:T(8,128)(2,1)S(1)}, bf16[2048,352]{0,1:T(8,128)(2,1)}, u32[]{:S(2)}) copy-start(bf16[2048,352]{0,1:T(8,128)(2,1)} %param.47) | copy-start | bytes 4325380
Sparse Core Ops, SparseCore 0:
  59.3 16.3 all-reduce.1
  240.4 56.5 reduce-scatter.1
